TPU v7x, 32 devices: a whole 2x2x4 slice. The times are simulated.
32 devices in a mesh: ep: 8 (over z, core), tp: 4 (over y, x).
Axes of the slice: x: 2, y: 2, z: 4, core: 2. Of those that a mesh axis runs over, the one named last changes fastest.
Arguments:
- tokens: bfloat16 [1024, 3072], P('ep', 'tp'), may hold values from -6 to 6
- routes: int32 [1024, 2], P('ep'), may hold values from 0 to 7, all different within a row; in each aligned block of 128 rows (0 to 127, 128 to 255, ...) at most 40 rows name the same one
- gates: float32 [1024, 2], P('ep'), may hold values from 0.1 to 1.5
- cotangent: bfloat16 [1024, 3072], P('ep', 'tp'), may hold values from -6 to 6
- w_gate: bfloat16 [8, 3072, 896], P('ep', 'tp'), may hold values from -0.109375 to 0.109375
- w_up: bfloat16 [8, 3072, 896], P('ep', 'tp'), may hold values from -0.109375 to 0.109375
- w_down: bfloat16 [8, 3072, 896], P('ep', 'tp'), may hold values from -0.1875 to 0.1875
- shared_hidden: bfloat16 [1024, 448], P('ep'), may hold values from -0.2362278 to 0.2362278
Outputs:
- token_grad: bfloat16 [1024, 3072], P('ep', 'tp')
- gate_grad: float32 [1024, 2], P('ep')
- grad_w_gate: float32 [8, 3072, 896], P('ep', 'tp')
- grad_w_up: float32 [8, 3072, 896], P('ep', 'tp')
- grad_w_down: float32 [8, 3072, 896], P('ep', 'tp')
- row_norms: float32 [3, 8, 3072], P(None, 'ep', 'tp')
- grad_shared: float32 [3072, 448], P('tp', 'ep')
- shared_norms: float32 [3072], P('tp')
Inputs may be any that keep to these rules, and one draw needn't show every extreme that they name: `routes`: in each aligned block of 128 rows (the tokens of one index of ep) a row names 2 different experts and no expert is named by more than 40 rows; some expert is named by exactly 40 rows in some blocks.
All inputs are finite; a program needn't handle non-finite values.
Results may differ from a plain program's by a relative error of at most 0.024.
Values may be sent and summed in bfloat16 or wider, within the bound.
A program may use at most 64 MiB of HBM per device.

v0:
```python
import jax
import jax.numpy as jnp
from jax import lax
from jax.sharding import PartitionSpec as P


def slot_targets(routes, experts, capacity):
    chosen = routes.reshape(-1)
    onehot = (chosen[:, None] == jnp.arange(experts, dtype=jnp.int32)[None, :]).astype(jnp.int32)
    earlier = jnp.cumsum(onehot, axis=0) - onehot
    position = jnp.sum(earlier * onehot, axis=1)
    return chosen * capacity + position


def expert_math(gate_sum, up_sum, down_sum):
    sigma = jax.nn.sigmoid(gate_sum)
    active = gate_sum * sigma
    hidden = (active * up_sum).astype(jnp.bfloat16)
    product = jnp.sum(active * up_sum * down_sum, axis=-1).astype(jnp.bfloat16)
    gate_back = (down_sum * up_sum * sigma * (1.0 + gate_sum * (1.0 - sigma))).astype(jnp.bfloat16)
    up_back = (down_sum * active).astype(jnp.bfloat16)
    return (hidden, gate_back, up_back, product)


def on_device(tokens, routes, gates, cotangent, w_gate, w_up, w_down, shared_hidden):
    tok_count, width_part = tokens.shape
    top_count = routes.shape[1]
    local_experts = w_gate.shape[0]
    experts = local_experts * lax.axis_size("ep")
    capacity = 5 * tok_count * top_count // (4 * experts)
    pair_count = tok_count * top_count
    target = slot_targets(routes, experts, capacity)
    source = (
        jnp.zeros((experts * capacity,), jnp.int32)
        .at[target]
        .set(jnp.arange(pair_count, dtype=jnp.int32))
    )
    filled = jnp.zeros((experts * capacity,), jnp.bool_).at[target].set(True)
    scaled = (gates[:, :, None] * cotangent[:, None, :].astype(jnp.float32)).astype(jnp.bfloat16)
    scaled = scaled.reshape(pair_count, width_part)
    zero_row = jnp.zeros((), jnp.bfloat16)
    token_rows = jnp.where(filled[:, None], tokens[source // top_count], zero_row)
    grad_rows = jnp.where(filled[:, None], scaled[source], zero_row)
    token_rows = token_rows.reshape(experts, capacity, width_part)
    grad_rows = grad_rows.reshape(experts, capacity, width_part)
    arrived_tok, arrived_grad = (
        lax.all_to_all(token_rows, "ep", split_axis=0, concat_axis=1, tiled=True),
        lax.all_to_all(grad_rows, "ep", split_axis=0, concat_axis=1, tiled=True),
    )
    gate_part = jnp.einsum("erd,edf->erf", arrived_tok, w_gate, preferred_element_type=jnp.float32)
    up_part = jnp.einsum("erd,edf->erf", arrived_tok, w_up, preferred_element_type=jnp.float32)
    down_part = jnp.einsum("erd,edf->erf", arrived_grad, w_down, preferred_element_type=jnp.float32)
    sums = (
        lax.psum(gate_part.astype(jnp.bfloat16), "tp").astype(jnp.float32),
        lax.psum(up_part.astype(jnp.bfloat16), "tp").astype(jnp.float32),
        lax.psum(down_part.astype(jnp.bfloat16), "tp").astype(jnp.float32),
    )
    hidden, gate_back, up_back, product = expert_math(sums[0], sums[1], sums[2])
    grad_gate = jnp.einsum(
        "erd,erf->edf", arrived_tok, gate_back, preferred_element_type=jnp.float32
    )
    grad_up = jnp.einsum("erd,erf->edf", arrived_tok, up_back, preferred_element_type=jnp.float32)
    grad_down = jnp.einsum("erd,erf->edf", arrived_grad, hidden, preferred_element_type=jnp.float32)
    token_back = jnp.einsum(
        "erf,edf->erd", gate_back, w_gate, preferred_element_type=jnp.float32
    ) + jnp.einsum("erf,edf->erd", up_back, w_up, preferred_element_type=jnp.float32)
    token_back = token_back.astype(jnp.bfloat16)
    back_rows, back_product = (
        lax.all_to_all(token_back, "ep", split_axis=1, concat_axis=0, tiled=True),
        lax.all_to_all(product, "ep", split_axis=1, concat_axis=0, tiled=True),
    )
    per_pair = back_rows.reshape(experts * capacity, width_part)[target]
    per_pair = per_pair.reshape(tok_count, top_count, width_part)
    token_grad = jnp.sum(per_pair.astype(jnp.float32), axis=1).astype(jnp.bfloat16)
    pair_product = back_product.reshape(experts * capacity)[target].reshape(tok_count, top_count)
    gate_grad = pair_product.astype(jnp.float32) / gates
    row_norms = jnp.stack(
        [
            jnp.sum(grad_gate * grad_gate, axis=-1),
            jnp.sum(grad_up * grad_up, axis=-1),
            jnp.sum(grad_down * grad_down, axis=-1),
        ],
        axis=0,
    )
    shared_term = jnp.einsum(
        "td,ts->ds", cotangent, shared_hidden, preferred_element_type=jnp.float32
    )
    grad_shared = lax.psum_scatter(shared_term, "ep", scatter_dimension=1, tiled=True)
    shared_norms = lax.psum(jnp.sum(grad_shared * grad_shared, axis=1), "ep")
    return (
        token_grad,
        gate_grad,
        grad_gate,
        grad_up,
        grad_down,
        row_norms,
        grad_shared,
        shared_norms,
    )


def solution(mesh):
    return jax.shard_map(
        on_device,
        mesh=mesh,
        in_specs=(
            P("ep", "tp"),
            P("ep", None),
            P("ep", None),
            P("ep", "tp"),
            P("ep", "tp", None),
            P("ep", "tp", None),
            P("ep", "tp", None),
            P("ep", None),
        ),
        out_specs=(
            P("ep", "tp"),
            P("ep", None),
            P("ep", "tp", None),
            P("ep", "tp", None),
            P("ep", "tp", None),
            P(None, "ep", "tp"),
            P("tp", "ep"),
            P("tp"),
        ),
        check_vma=False,
    )
```

profile of v0, /device:TPU:0, one launch (start us, length us, event | category | flops | bytes accessed | tf_op | source)
XLA Modules:
  0.0 189.0 jit_solution(876428887451017277)
XLA Ops:
  8.0 0.8 broadcast_multiply_fusion
  8.8 0.8 copy.30
  11.1 1.4 scatter_custom_fusion.1
  12.5 1.5 scatter_custom_fusion
  14.1 1.2 mul.83
  16.1 2.1 %gather_fusion.1 = bf16[320,768]{1,0:T(8,128)(2,1)S(1)} fusion(bf16[128,768]{1,0:T(8,128)(2,1)S(1)} %copy-done.1, s32[1024]{0:T(1024)S(1)} %get-tuple-element.45), kind=kCustom, calls=%fused_computation.1 | custom fusion | bytes 984320 | tf_op jit(solution)/shard_map/gather | solution.py:42
  18.4 2.1 %gather_fusion = bf16[320,768]{1,0:T(8,128)(2,1)S(1)} fusion(bf16[256,768]{1,0:T(8,128)(2,1)S(1)} %multiply_convert_fusion, s32[1024]{0:T(1024)S(1)} %get-tuple-element.46), kind=kCustom, calls=%fused_computation | custom fusion | bytes 984320 | tf_op jit(solution)/shard_map/gather | solution.py:43
  20.5 0.9 broadcast_select_fusion
  21.4 20.8 %all_to_all.17 = bf16[8,40,768]{2,1,0:T(8,128)(2,1)S(1)} all-to-all(bf16[8,40,768]{2,1,0:T(8,128)(2,1)S(1)} %get-tuple-element.37), channel_id=1, replica_groups=mesh['ep'=8,'tp'=4] {'ep'}, dimensions={0} | all-to-all | bytes 983040 | tf_op jit(solution)/shard_map/all_to_all | solution.py:47
  42.2 3.5 %all-to-all-start = ((bf16[8,40,768]{2,1,0:T(8,128)(2,1)}), bf16[8,40,768]{2,1,0:T(8,128)(2,1)S(1)}, u32[]{:S(2)}, u32[]{:S(2)}) async-start(bf16[8,40,768]{2,1,0:T(8,128)(2,1)} %get-tuple-element.38), calls=%async_computation | async-start | bytes 983040 | tf_op jit(solution)/shard_map/all_to_all | solution.py:48
  45.7 2.8 %fusion.28 = bf16[1,320,896]{2,1,0:T(8,128)(2,1)} fusion(bf16[320,768]{1,0:T(8,128)(2,1)S(1)} %bitcast.94, bf16[1,768,896]{2,1,0:T(8,128)(2,1)} %param.13), kind=kOutput, calls=%fused_computation.32 | convolution fusion | flops 440688640 | bytes 2441216 | tf_op jit(solution)/shard_map/erd,edf->erf/dot_general | solution.py:51
  48.6 1.5 fusion.25
  50.1 10.2 %all-to-all-done = bf16[8,40,768]{2,1,0:T(8,128)(2,1)S(1)} async-done(((bf16[8,40,768]{2,1,0:T(8,128)(2,1)}), bf16[8,40,768]{2,1,0:T(8,128)(2,1)S(1)}, u32[]{:S(2)}, u32[]{:S(2)}) %all-to-all-start) | async-done | bytes 491552 | tf_op jit(solution)/shard_map/all_to_all | solution.py:48
  60.2 3.0 %fusion.31 = bf16[1,320,896]{2,1,0:T(8,128)(2,1)} fusion(bf16[320,768]{1,0:T(8,128)(2,1)S(1)} %bitcast.98, bf16[1,768,896]{2,1,0:T(8,128)(2,1)} %param.14), kind=kOutput, calls=%fused_computation.33 | convolution fusion | flops 440688640 | bytes 2441216 | tf_op jit(solution)/shard_map/erd,edf->erf/dot_general | solution.py:52
  63.3 0.8 copy-done.2
  64.2 1.4 fusion.68
  65.7 60.3 %all-reduce.3.cloned.1.call-done = (bf16[1,320,896]{2,1,0:T(8,128)(2,1)}, bf16[1,320,896]{2,1,0:T(8,128)(2,1)}, bf16[1,320,896]{2,1,0:T(8,128)(2,1)}) async-done(((bf16[1,320,896]{2,1,0:T(8,128)(2,1)}, bf16[1,320,896]{2,1,0:T(8,128)(2,1)}, bf16[1,320,896]{2,1,0:T(8,128)(2,1)}), (bf16[1,320,896]{2,1,0:T(8,128)(2,1)}, bf16[1,320,896]{2,1,0:T(8,128)(2,1)}, ...) | async-done | bytes 1720336 | tf_op jit(solution)/shard_map/psum | solution.py:56
  125.9 2.0 %fusion.41 = bf16[320]{0:T(512)(128)(2,1)S(1)} fusion(bf16[1,320,896]{2,1,0:T(8,128)(2,1)} %get-tuple-element.32, bf16[1,320,896]{2,1,0:T(8,128)(2,1)} %get-tuple-element.33, bf16[1,320,896]{2,1,0:T(8,128)(2,1)} %get-tuple-element.34), kind=kLoop, calls=%fused_computation.39 | loop fusion | flops 2866880 | bytes 1720960 | tf_op jit(solution)/shard_map/reduce_sum | solution.py:19
  128.7 4.6 %all-to-all-start.3 = ((bf16[1,8,40]{2,0,1:T(2,128)(2,1)}), bf16[1,8,40]{2,0,1:T(2,128)(2,1)S(1)}, u32[]{:S(2)}, u32[]{:S(2)}) async-start(bf16[1,8,40]{2,0,1:T(2,128)(2,1)} %convert_element_type.103), calls=%async_computation.3 | async-start | bytes 8192 | tf_op jit(solution)/shard_map/all_to_all | solution.py:70
  133.3 1.0 fusion
  134.7 0.9 fusion.34
  135.7 2.6 %multiply_reduce_fusion = (f32[768]{0:T(1024)S(1)}, f32[768,896]{1,0:T(8,128)}) fusion(bf16[320,768]{1,0:T(8,128)(2,1)S(1)} %bitcast.99, bf16[1,320,896]{2,1,0:T(8,128)(2,1)S(1)} %copy-done.5, bf16[1,320,896]{2,1,0:T(8,128)(2,1)S(1)} %copy-done.7), kind=kOutput, calls=%fused_computation.6 | convolution fusion | flops 444071168 | bytes 4393984 | tf_op jit(solution)/shard_map/erd,erf->edf/dot_general | solution.py:63
  139.6 3.7 %reduce.11 = bf16[320,768]{1,0:T(8,128)(2,1)S(1)} reduce(bf16[320,1,768]{2,1,0:T(2,128)(2,1)S(1)} %bitcast.90, bf16[]{:T(256)} %broadcast.119), dimensions={1}, to_apply=%bitcast.88.reduce_sub_computation | reduce | bytes 983042
  143.3 0.9 reshape.256
  144.2 5.1 %all-to-all-start.2 = ((bf16[8,2,15360]{2,1,0:T(2,128)(2,1)}), bf16[8,2,15360]{2,1,0:T(2,128)(2,1)S(1)}, u32[]{:S(2)}, u32[]{:S(2)}) async-start(bf16[8,2,15360]{2,1,0:T(2,128)(2,1)} %reshape.256), calls=%async_computation.2 | async-start | bytes 983040 | tf_op jit(solution)/shard_map/all_to_all | solution.py:69
  149.4 3.8 %multiply_reduce_fusion.1 = (f32[768]{0:T(1024)S(1)}, f32[768,896]{1,0:T(8,128)}) fusion(bf16[320,768]{1,0:T(8,128)(2,1)S(1)} %bitcast.96, bf16[1,320,896]{2,1,0:T(8,128)(2,1)S(1)} %copy-done.4, bf16[1,320,896]{2,1,0:T(8,128)(2,1)} %get-tuple-element.34), kind=kOutput, calls=%fused_computation.7 | convolution fusion | flops 444071168 | bytes 4393984 | tf_op jit(solution)/shard_map/erd,erf->edf/dot_general | solution.py:62
  153.2 2.7 %multiply_reduce_fusion.2 = (f32[768]{0:T(1024)S(1)}, f32[768,896]{1,0:T(8,128)}) fusion(bf16[320,768]{1,0:T(8,128)(2,1)S(1)} %bitcast.97, bf16[1,320,896]{2,1,0:T(8,128)(2,1)S(1)} %copy-done.8, bf16[1,320,896]{2,1,0:T(8,128)(2,1)S(1)} %copy-done.6, bf16[1,320,896]{2,1,0:T(8,128)(2,1)S(1)} %copy-done.4), kind=kOutput, calls=%fused_computation.8 | convolution fusion | flops 445504768 | bytes 4967424 | tf_op jit(solution)/shard_map/erd,erf->edf/dot_general | solution.py:59
  156.6 1.9 %gather_fusion.3 = bf16[256]{0:T(256)(128)(2,1)S(1)} fusion(bf16[320]{0:T(512)(128)(2,1)S(1)} %reshape.197, s32[1024]{0:T(1024)S(1)} %pad_clamp_fusion), kind=kCustom, calls=%fused_computation.3 | custom fusion | bytes 2048 | tf_op jit(solution)/shard_map/gather | solution.py:75
  159.4 0.9 multiply_reduce_fusion.3
  160.3 17.7 %psum.31 = f32[768]{0:T(1024)} all-reduce(f32[768]{0:T(1024)S(1)} %multiply_reduce_fusion.3), channel_id=1, replica_groups=mesh['ep'=8,'tp'=4] {'ep'}, use_global_device_ids=true, to_apply=%region_15.16 | all-reduce | flops 768 | bytes 6144 | tf_op jit(solution)/shard_map/psum | solution.py:89
  178.5 1.2 gather_fusion.2
  179.8 1.7 reduce_sum.70
  (74 shorter events, 7.3 us)
Async XLA Ops:
  8.0 40.6 %copy-start = (bf16[1,768,896]{2,1,0:T(8,128)(2,1)S(1)}, bf16[1,768,896]{2,1,0:T(8,128)(2,1)}, u32[]{:S(2)}) copy-start(bf16[1,768,896]{2,1,0:T(8,128)(2,1)} %param.12) | copy-start | bytes 4128772
  14.1 1.7 copy-start.14
  14.1 2.0 %copy-start.1 = (bf16[128,768]{1,0:T(8,128)(2,1)S(1)}, bf16[128,768]{1,0:T(8,128)(2,1)}, u32[]{:S(2)}) copy-start(bf16[128,768]{1,0:T(8,128)(2,1)} %param.8) | copy-start | bytes 589828
  42.2 6.4 %copy-start.9 = (bf16[8,40,768]{2,1,0:T(8,128)(2,1)}, bf16[8,40,768]{2,1,0:T(8,128)(2,1)S(1)}, u32[]{:S(2)}) copy-start(bf16[8,40,768]{2,1,0:T(8,128)(2,1)S(1)} %all_to_all.17) | copy-start | bytes 1474564
  42.2 18.0 %all-to-all-start = ((bf16[8,40,768]{2,1,0:T(8,128)(2,1)}), bf16[8,40,768]{2,1,0:T(8,128)(2,1)S(1)}, u32[]{:S(2)}, u32[]{:S(2)}) async-start(bf16[8,40,768]{2,1,0:T(8,128)(2,1)} %get-tuple-element.38), calls=%async_computation | async-start | bytes 983040 | tf_op jit(solution)/shard_map/all_to_all | solution.py:48
  45.7 80.2 %all-reduce.3.cloned.1.call-start = ((), (), s32[]{:S(2)}) async-start(), calls=%async_computation.6 | async-start | bytes 3440640 | tf_op jit(solution)/shard_map/psum | solution.py:56
  60.2 3.0 %copy-start.11 = (bf16[8,40,768]{2,1,0:T(8,128)(2,1)}, bf16[8,40,768]{2,1,0:T(8,128)(2,1)S(1)}, u32[]{:S(2)}) copy-start(bf16[8,40,768]{2,1,0:T(8,128)(2,1)S(1)} %all-to-all-done) | copy-start | bytes 1474564
  63.3 0.9 copy-start.2
  63.3 1.0 copy-start.13
  63.3 96.1 %reduce-scatter.2.cloned.1.call-start = ((), (), s32[]{:S(2)}) async-start(), calls=%async_computation.5 | async-start | bytes 1548288 | tf_op jit(solution)/shard_map/reduce_scatter | solution.py:88
  125.9 7.3 %copy-start.3 = (bf16[1,320,896]{2,1,0:T(8,128)(2,1)S(1)}, bf16[1,320,896]{2,1,0:T(8,128)(2,1)}, u32[]{:S(2)}) copy-start(bf16[1,320,896]{2,1,0:T(8,128)(2,1)} %get-tuple-element.32) | copy-start | bytes 1720324
  125.9 7.3 %copy-start.5 = (bf16[1,320,896]{2,1,0:T(8,128)(2,1)S(1)}, bf16[1,320,896]{2,1,0:T(8,128)(2,1)}, u32[]{:S(2)}) copy-start(bf16[1,320,896]{2,1,0:T(8,128)(2,1)} %get-tuple-element.33) | copy-start | bytes 1720324
  125.9 7.4 %copy-start.7 = (bf16[1,320,896]{2,1,0:T(8,128)(2,1)S(1)}, bf16[1,320,896]{2,1,0:T(8,128)(2,1)}, u32[]{:S(2)}) copy-start(bf16[1,320,896]{2,1,0:T(8,128)(2,1)} %get-tuple-element.34) | copy-start | bytes 1720324
  128.7 15.6 %all-to-all-start.3 = ((bf16[1,8,40]{2,0,1:T(2,128)(2,1)}), bf16[1,8,40]{2,0,1:T(2,128)(2,1)S(1)}, u32[]{:S(2)}, u32[]{:S(2)}) async-start(bf16[1,8,40]{2,0,1:T(2,128)(2,1)} %convert_element_type.103), calls=%async_computation.3 | async-start | bytes 8192 | tf_op jit(solution)/shard_map/all_to_all | solution.py:70
  133.3 1.3 copy-start.15
  134.7 1.0 copy-start.12
  143.3 6.0 %copy-start.4 = (bf16[1,320,896]{2,1,0:T(8,128)(2,1)S(1)}, bf16[1,320,896]{2,1,0:T(8,128)(2,1)}, u32[]{:S(2)}) copy-start(bf16[1,320,896]{2,1,0:T(8,128)(2,1)} %get-tuple-element.32) | copy-start | bytes 1720324
  143.3 6.0 %copy-start.10 = (bf16[8,40,768]{2,1,0:T(8,128)(2,1)S(1)}, bf16[8,40,768]{2,1,0:T(8,128)(2,1)}, u32[]{:S(2)}) copy-start(bf16[8,40,768]{2,1,0:T(8,128)(2,1)} %copy-done.9) | copy-start | bytes 1474564
  144.2 33.8 %all-to-all-start.2 = ((bf16[8,2,15360]{2,1,0:T(2,128)(2,1)}), bf16[8,2,15360]{2,1,0:T(2,128)(2,1)S(1)}, u32[]{:S(2)}, u32[]{:S(2)}) async-start(bf16[8,2,15360]{2,1,0:T(2,128)(2,1)} %reshape.256), calls=%async_computation.2 | async-start | bytes 983040 | tf_op jit(solution)/shard_map/all_to_all | solution.py:69
  149.4 3.8 %copy-start.6 = (bf16[1,320,896]{2,1,0:T(8,128)(2,1)S(1)}, bf16[1,320,896]{2,1,0:T(8,128)(2,1)}, u32[]{:S(2)}) copy-start(bf16[1,320,896]{2,1,0:T(8,128)(2,1)} %get-tuple-element.33) | copy-start | bytes 1720324
  149.4 3.8 %copy-start.8 = (bf16[1,320,896]{2,1,0:T(8,128)(2,1)S(1)}, bf16[1,320,896]{2,1,0:T(8,128)(2,1)}, u32[]{:S(2)}) copy-start(bf16[1,320,896]{2,1,0:T(8,128)(2,1)} %get-tuple-element.34) | copy-start | bytes 1720324
Sparse Core Ops, SparseCore 0:
  63.4 62.4 all-reduce.2
Sparse Core Ops, SparseCore 1:
  66.6 32.3 reduce-scatter.1
where the time goes:
time: 190 us; the launch traced here: 189 us
  waiting for transfers between devices  70.5 us (37%)
  blocking collectives  38.5 us (20%)
  matrix products  19.8 us (10%)
  local copies, waits for them, and re-layouts  19.6 us (10%)
  between operations  15.8 us (8%)
  starting transfers between devices  13.3 us (7%)
  other arithmetic  11.7 us (6%)
    psum x1, waiting for transfers between devices, on_device(): lax.psum(down_part.astype(jnp.bfloat16), 'tp').astype(jnp.float32)  60.3 us
    all_to_all x1, blocking collectives, on_device(): lax.all_to_all(token_rows, 'ep', split_axis=0, concat_axis=1, tiled=True)  20.8 us
    psum x1, blocking collectives, on_device(): shared_norms = lax.psum(jnp.sum(grad_shared * grad_shared, axis=1), 'ep')  17.7 us
    all_to_all x1, waiting for transfers between devices, on_device(): lax.all_to_all(grad_rows, 'ep', split_axis=0, concat_axis=1, tiled=True)  10.2 us
    all_to_all x1, starting transfers between devices, on_device(): lax.all_to_all(token_back, 'ep', split_axis=1, concat_axis=0, tiled=True)  5.09 us
    unnamed x39, local copies, waits for them, and re-layouts  4.82 us
    all_to_all x1, starting transfers between devices, on_device(): lax.all_to_all(product, 'ep', split_axis=1, concat_axis=0, tiled=True)  4.61 us
  transfers between devices with their start and end apart: 5, of which 2 were waited for; matrix products, arithmetic and copies ran while one was open for 16% of the time, Pallas kernels for 0%

commit v1 on v0

--- a/solution.py
+++ b/solution.py
@@ -45,7 +45,12 @@
     grad_rows = grad_rows.reshape(experts, capacity, width_part)
     arrived_tok, arrived_grad = (
         lax.all_to_all(token_rows, "ep", split_axis=0, concat_axis=1, tiled=True),
-        lax.all_to_all(grad_rows, "ep", split_axis=0, concat_axis=1, tiled=True),
+        jnp.concatenate(
+            lax.all_to_all(
+                jnp.stack(jnp.split(grad_rows, lax.axis_size("ep"), axis=0)), "ep", 0, 0
+            ),
+            axis=1,
+        ),
     )
     gate_part = jnp.einsum("erd,edf->erf", arrived_tok, w_gate, preferred_element_type=jnp.float32)
     up_part = jnp.einsum("erd,edf->erf", arrived_tok, w_up, preferred_element_type=jnp.float32)

time: 190 us -> 187 us (0.984)
  blocking collectives: 38.5 us -> 17.7 us
  starting transfers between devices: 13.3 us -> 19.6 us
  local copies, waits for them, and re-layouts: 19.6 us -> 24.2 us
  waiting for transfers between devices: 70.5 us -> 75 us
  matrix products: 19.8 us -> 21.9 us
    all_to_all x1 -> x0, blocking collectives: 20.8 us -> none  [on_device(): lax.all_to_all(token_rows, 'ep', split_axis=0, concat_axis=1, tiled=True)]
    all_to_all x1 -> x2, starting transfers between devices: 3.48 us -> 9.84 us  [the longest x1 6.35 us: on_device(): lax.all_to_all(token_rows, 'ep', split_axis=0, concat_axis=1, tiled=True)]
    unnamed x39 -> x44, local copies, waits for them, and re-layouts: 4.82 us -> 9.74 us
    all_to_all x1 -> x2, waiting for transfers between devices: 10.2 us -> 14.7 us  [the longest x1 9 us: on_device(): lax.all_to_all(jnp.stack(jnp.split(grad_rows, lax.axis_size('ep'), axis=0...]
  transfers between devices with their start and end apart: 5 -> 6, of which waited for: 2 -> 3; matrix products, arithmetic and copies ran while one was open for 16% -> 22% of each run, Pallas kernels for 0% -> 0%
where the time goes in v1:
time: 187 us; the launch traced here: 186 us
  waiting for transfers between devices  75 us (40%)
  local copies, waits for them, and re-layouts  24.2 us (13%)
  matrix products  21.9 us (12%)
  starting transfers between devices  19.6 us (10%)
  blocking collectives  17.7 us (9%)
  between operations  15.8 us (8%)
  other arithmetic  11.8 us (6%)
    psum x1, waiting for transfers between devices, on_device(): lax.psum(down_part.astype(jnp.bfloat16), 'tp').astype(jnp.float32)  60.3 us
    psum x1, blocking collectives, on_device(): shared_norms = lax.psum(jnp.sum(grad_shared * grad_shared, axis=1), 'ep')  17.7 us
    unnamed x44, local copies, waits for them, and re-layouts  9.74 us
    all_to_all x1, waiting for transfers between devices, on_device(): lax.all_to_all(jnp.stack(jnp.split(grad_rows, lax.axis_size('ep'), axis=0...  9 us
    all_to_all x1, starting transfers between devices, on_device(): lax.all_to_all(token_rows, 'ep', split_axis=0, concat_axis=1, tiled=True)  6.35 us
    all_to_all x1, waiting for transfers between devices, on_device(): lax.all_to_all(token_rows, 'ep', split_axis=0, concat_axis=1, tiled=True)  5.66 us
    all_to_all x1, starting transfers between devices, on_device(): lax.all_to_all(token_back, 'ep', split_axis=1, concat_axis=0, tiled=True)  5.09 us
    all_to_all x1, starting transfers between devices, on_device(): lax.all_to_all(product, 'ep', split_axis=1, concat_axis=0, tiled=True)  4.61 us
  transfers between devices with their start and end apart: 6, of which 3 were waited for; matrix products, arithmetic and copies ran while one was open for 22% of the time, Pallas kernels for 0%

profile of v1, /device:TPU:0, one launch (start us, length us, event | category | flops | bytes accessed | tf_op | source)
XLA Modules:
  0.0 186.1 jit_solution(642323159309392584)
XLA Ops:
  8.0 0.8 broadcast_multiply_fusion
  8.8 0.8 copy.30
  11.1 1.4 scatter_custom_fusion.1
  12.6 1.5 scatter_custom_fusion
  14.2 2.1 %gather_fusion.1 = bf16[320,768]{1,0:T(8,128)(2,1)S(1)} fusion(bf16[128,768]{1,0:T(8,128)(2,1)S(1)} %copy-done.1, s32[1024]{0:T(1024)S(1)} %get-tuple-element.43), kind=kCustom, calls=%fused_computation.1 | custom fusion | bytes 984320 | tf_op jit(solution)/shard_map/gather | solution.py:42
  16.3 0.9 broadcast_select_fusion.1
  17.2 6.4 %all-to-all-start.1 = ((bf16[8,40,768]{2,1,0:T(8,128)(2,1)}), bf16[8,40,768]{2,1,0:T(8,128)(2,1)}, u32[]{:S(2)}, u32[]{:S(2)}) async-start(bf16[8,40,768]{2,1,0:T(8,128)(2,1)} %broadcast_select_fusion.1), calls=%async_computation.1 | async-start | bytes 983040 | tf_op jit(solution)/shard_map/all_to_all | solution.py:47
  25.3 2.1 %gather_fusion = bf16[320,768]{1,0:T(8,128)(2,1)S(1)} fusion(bf16[256,768]{1,0:T(8,128)(2,1)S(1)} %multiply_convert_fusion, s32[1024]{0:T(1024)S(1)} %get-tuple-element.44), kind=kCustom, calls=%fused_computation | custom fusion | bytes 984320 | tf_op jit(solution)/shard_map/gather | solution.py:43
  32.6 5.7 %all-to-all-done.1 = bf16[8,40,768]{2,1,0:T(8,128)(2,1)} async-done(((bf16[8,40,768]{2,1,0:T(8,128)(2,1)}), bf16[8,40,768]{2,1,0:T(8,128)(2,1)}, u32[]{:S(2)}, u32[]{:S(2)}) %all-to-all-start.1) | async-done | bytes 491552 | tf_op jit(solution)/shard_map/all_to_all | solution.py:47
  38.3 3.5 %all-to-all-start = ((bf16[8,1,40,768]{3,2,1,0:T(8,128)(2,1)}), bf16[8,1,40,768]{3,2,1,0:T(8,128)(2,1)S(1)}, u32[]{:S(2)}, u32[]{:S(2)}) async-start(bf16[8,1,40,768]{3,2,1,0:T(8,128)(2,1)} %fusion.54), calls=%async_computation | async-start | bytes 983040 | tf_op jit(solution)/shard_map/all_to_all | solution.py:49
  41.8 3.0 %fusion.28 = bf16[1,320,896]{2,1,0:T(8,128)(2,1)} fusion(bf16[320,768]{1,0:T(8,128)(2,1)} %bitcast.16, bf16[1,768,896]{2,1,0:T(8,128)(2,1)} %param.13), kind=kOutput, calls=%fused_computation.32 | convolution fusion | flops 440688640 | bytes 2441216 | tf_op jit(solution)/shard_map/erd,edf->erf/dot_general | solution.py:56
  44.8 2.5 %fusion.25 = bf16[1,320,896]{2,1,0:T(8,128)(2,1)} fusion(bf16[320,768]{1,0:T(8,128)(2,1)} %bitcast.16, bf16[1,768,896]{2,1,0:T(8,128)(2,1)S(1)} %copy-done), kind=kOutput, calls=%fused_computation.31 | convolution fusion | flops 440688640 | bytes 2441216 | tf_op jit(solution)/shard_map/erd,edf->erf/dot_general | solution.py:55
  47.3 9.0 %all-to-all-done = bf16[8,1,40,768]{3,2,1,0:T(8,128)(2,1)S(1)} async-done(((bf16[8,1,40,768]{3,2,1,0:T(8,128)(2,1)}), bf16[8,1,40,768]{3,2,1,0:T(8,128)(2,1)S(1)}, u32[]{:S(2)}, u32[]{:S(2)}) %all-to-all-start) | async-done | bytes 491552 | tf_op jit(solution)/shard_map/all_to_all | solution.py:49
  56.3 3.0 %fusion.31 = bf16[1,320,896]{2,1,0:T(8,128)(2,1)} fusion(bf16[320,768]{1,0:T(8,128)(2,1)S(1)} %bitcast.124, bf16[1,768,896]{2,1,0:T(8,128)(2,1)} %param.14), kind=kOutput, calls=%fused_computation.33 | convolution fusion | flops 440688640 | bytes 2441216 | tf_op jit(solution)/shard_map/erd,edf->erf/dot_general | solution.py:57
  59.4 0.8 copy-done.12
  60.2 1.4 fusion.76
  61.7 60.3 %all-reduce.3.cloned.1.call-done = (bf16[1,320,896]{2,1,0:T(8,128)(2,1)}, bf16[1,320,896]{2,1,0:T(8,128)(2,1)}, bf16[1,320,896]{2,1,0:T(8,128)(2,1)}) async-done(((bf16[1,320,896]{2,1,0:T(8,128)(2,1)}, bf16[1,320,896]{2,1,0:T(8,128)(2,1)}, bf16[1,320,896]{2,1,0:T(8,128)(2,1)}), (bf16[1,320,896]{2,1,0:T(8,128)(2,1)}, bf16[1,320,896]{2,1,0:T(8,128)(2,1)}, ...) | async-done | bytes 1720336 | tf_op jit(solution)/shard_map/psum | solution.py:61
  122.0 2.0 %fusion.41 = bf16[320]{0:T(512)(128)(2,1)S(1)} fusion(bf16[1,320,896]{2,1,0:T(8,128)(2,1)} %get-tuple-element.32, bf16[1,320,896]{2,1,0:T(8,128)(2,1)} %get-tuple-element.33, bf16[1,320,896]{2,1,0:T(8,128)(2,1)} %get-tuple-element.34), kind=kLoop, calls=%fused_computation.39 | loop fusion | flops 2866880 | bytes 1720960 | tf_op jit(solution)/shard_map/reduce_sum | solution.py:19
  124.8 4.6 %all-to-all-start.3 = ((bf16[1,8,40]{2,0,1:T(2,128)(2,1)}), bf16[1,8,40]{2,0,1:T(2,128)(2,1)S(1)}, u32[]{:S(2)}, u32[]{:S(2)}) async-start(bf16[1,8,40]{2,0,1:T(2,128)(2,1)} %convert_element_type.103), calls=%async_computation.3 | async-start | bytes 8192 | tf_op jit(solution)/shard_map/all_to_all | solution.py:75
  129.4 1.0 fusion
  130.7 0.9 fusion.34
  131.8 2.6 %multiply_reduce_fusion = (f32[768]{0:T(1024)S(1)}, f32[768,896]{1,0:T(8,128)}) fusion(bf16[320,768]{1,0:T(8,128)(2,1)S(1)} %bitcast.125, bf16[1,320,896]{2,1,0:T(8,128)(2,1)S(1)} %copy-done.7, bf16[1,320,896]{2,1,0:T(8,128)(2,1)S(1)} %copy-done.9), kind=kOutput, calls=%fused_computation.6 | convolution fusion | flops 444071168 | bytes 4393984 | tf_op jit(solution)/shard_map/erd,erf->edf/dot_general | solution.py:68
  135.7 3.7 %reduce.11 = bf16[320,768]{1,0:T(8,128)(2,1)S(1)} reduce(bf16[320,1,768]{2,1,0:T(2,128)(2,1)S(1)} %bitcast.121, bf16[]{:T(256)} %broadcast.117), dimensions={1}, to_apply=%bitcast.119.reduce_sub_computation | reduce | bytes 983042
  139.4 0.9 reshape.264
  140.3 5.1 %all-to-all-start.2 = ((bf16[8,2,15360]{2,1,0:T(2,128)(2,1)}), bf16[8,2,15360]{2,1,0:T(2,128)(2,1)S(1)}, u32[]{:S(2)}, u32[]{:S(2)}) async-start(bf16[8,2,15360]{2,1,0:T(2,128)(2,1)} %reshape.264), calls=%async_computation.2 | async-start | bytes 983040 | tf_op jit(solution)/shard_map/all_to_all | solution.py:74
  145.4 3.7 %multiply_reduce_fusion.1 = (f32[768]{0:T(1024)S(1)}, f32[768,896]{1,0:T(8,128)}) fusion(bf16[320,768]{1,0:T(8,128)(2,1)} %bitcast.16, bf16[1,320,896]{2,1,0:T(8,128)(2,1)S(1)} %copy-done.6, bf16[1,320,896]{2,1,0:T(8,128)(2,1)S(1)} %copy-done.9), kind=kOutput, calls=%fused_computation.7 | convolution fusion | flops 444071168 | bytes 4393984 | tf_op jit(solution)/shard_map/erd,erf->edf/dot_general | solution.py:67
  149.1 3.8 %multiply_reduce_fusion.2 = (f32[768]{0:T(1024)S(1)}, f32[768,896]{1,0:T(8,128)}) fusion(bf16[320,768]{1,0:T(8,128)(2,1)} %bitcast.16, bf16[1,320,896]{2,1,0:T(8,128)(2,1)S(1)} %copy-done.9, bf16[1,320,896]{2,1,0:T(8,128)(2,1)S(1)} %copy-done.8, bf16[1,320,896]{2,1,0:T(8,128)(2,1)S(1)} %copy-done.6), kind=kOutput, calls=%fused_computation.8 | convolution fusion | flops 445504768 | bytes 4967424 | tf_op jit(solution)/shard_map/erd,erf->edf/dot_general | solution.py:64
  153.6 1.9 %gather_fusion.3 = bf16[256]{0:T(256)(128)(2,1)S(1)} fusion(bf16[320]{0:T(512)(128)(2,1)S(1)} %reshape.205, s32[1024]{0:T(1024)S(1)} %pad_clamp_fusion), kind=kCustom, calls=%fused_computation.3 | custom fusion | bytes 2048 | tf_op jit(solution)/shard_map/gather | solution.py:80
  156.4 0.9 multiply_reduce_fusion.3
  157.4 17.7 %psum.31 = f32[768]{0:T(1024)} all-reduce(f32[768]{0:T(1024)S(1)} %multiply_reduce_fusion.3), channel_id=1, replica_groups=mesh['ep'=8,'tp'=4] {'ep'}, use_global_device_ids=true, to_apply=%region_15.16 | all-reduce | flops 768 | bytes 6144 | tf_op jit(solution)/shard_map/psum | solution.py:94
  175.6 1.2 gather_fusion.2
  176.9 1.7 reduce_sum.70
  (82 shorter events, 13.2 us)
Async XLA Ops:
  8.0 36.8 %copy-start = (bf16[1,768,896]{2,1,0:T(8,128)(2,1)S(1)}, bf16[1,768,896]{2,1,0:T(8,128)(2,1)}, u32[]{:S(2)}) copy-start(bf16[1,768,896]{2,1,0:T(8,128)(2,1)} %param.12) | copy-start | bytes 4128772
  8.0 6.1 %copy-start.1 = (bf16[128,768]{1,0:T(8,128)(2,1)S(1)}, bf16[128,768]{1,0:T(8,128)(2,1)}, u32[]{:S(2)}) copy-start(bf16[128,768]{1,0:T(8,128)(2,1)} %param.8) | copy-start | bytes 589828
  16.3 7.3 %copy-start.2 = (bf16[128,768]{1,0:T(8,128)(2,1)S(1)}, bf16[128,768]{1,0:T(8,128)(2,1)}, u32[]{:S(2)}) copy-start(bf16[128,768]{1,0:T(8,128)(2,1)} %param.11) | copy-start | bytes 589828
  17.2 21.1 %all-to-all-start.1 = ((bf16[8,40,768]{2,1,0:T(8,128)(2,1)}), bf16[8,40,768]{2,1,0:T(8,128)(2,1)}, u32[]{:S(2)}, u32[]{:S(2)}) async-start(bf16[8,40,768]{2,1,0:T(8,128)(2,1)} %broadcast_select_fusion.1), calls=%async_computation.1 | async-start | bytes 983040 | tf_op jit(solution)/shard_map/all_to_all | solution.py:47
  23.6 0.8 copy-start.13
  24.5 0.6 copy-start.3
  38.3 18.0 %all-to-all-start = ((bf16[8,1,40,768]{3,2,1,0:T(8,128)(2,1)}), bf16[8,1,40,768]{3,2,1,0:T(8,128)(2,1)S(1)}, u32[]{:S(2)}, u32[]{:S(2)}) async-start(bf16[8,1,40,768]{3,2,1,0:T(8,128)(2,1)} %fusion.54), calls=%async_computation | async-start | bytes 983040 | tf_op jit(solution)/shard_map/all_to_all | solution.py:49
  41.8 80.2 %all-reduce.3.cloned.1.call-start = ((), (), s32[]{:S(2)}) async-start(), calls=%async_computation.6 | async-start | bytes 3440640 | tf_op jit(solution)/shard_map/psum | solution.py:61
  56.3 3.0 %copy-start.10 = (bf16[8,1,40,768]{3,2,1,0:T(8,128)(2,1)}, bf16[8,1,40,768]{3,2,1,0:T(8,128)(2,1)S(1)}, u32[]{:S(2)}) copy-start(bf16[8,1,40,768]{3,2,1,0:T(8,128)(2,1)S(1)} %all-to-all-done) | copy-start | bytes 1474564
  59.3 0.9 copy-start.12
  59.4 97.0 %reduce-scatter.2.cloned.1.call-start = ((), (), s32[]{:S(2)}) async-start(), calls=%async_computation.5 | async-start | bytes 1548288 | tf_op jit(solution)/shard_map/reduce_scatter | solution.py:93
  122.0 7.3 %copy-start.5 = (bf16[1,320,896]{2,1,0:T(8,128)(2,1)S(1)}, bf16[1,320,896]{2,1,0:T(8,128)(2,1)}, u32[]{:S(2)}) copy-start(bf16[1,320,896]{2,1,0:T(8,128)(2,1)} %get-tuple-element.32) | copy-start | bytes 1720324
  122.0 7.3 %copy-start.7 = (bf16[1,320,896]{2,1,0:T(8,128)(2,1)S(1)}, bf16[1,320,896]{2,1,0:T(8,128)(2,1)}, u32[]{:S(2)}) copy-start(bf16[1,320,896]{2,1,0:T(8,128)(2,1)} %get-tuple-element.33) | copy-start | bytes 1720324
  122.0 7.4 %copy-start.9 = (bf16[1,320,896]{2,1,0:T(8,128)(2,1)S(1)}, bf16[1,320,896]{2,1,0:T(8,128)(2,1)}, u32[]{:S(2)}) copy-start(bf16[1,320,896]{2,1,0:T(8,128)(2,1)} %get-tuple-element.34) | copy-start | bytes 1720324
  124.8 15.6 %all-to-all-start.3 = ((bf16[1,8,40]{2,0,1:T(2,128)(2,1)}), bf16[1,8,40]{2,0,1:T(2,128)(2,1)S(1)}, u32[]{:S(2)}, u32[]{:S(2)}) async-start(bf16[1,8,40]{2,0,1:T(2,128)(2,1)} %convert_element_type.103), calls=%async_computation.3 | async-start | bytes 8192 | tf_op jit(solution)/shard_map/all_to_all | solution.py:75
  129.4 1.3 copy-start.14
  130.7 1.0 copy-start.11
  139.4 6.0 %copy-start.6 = (bf16[1,320,896]{2,1,0:T(8,128)(2,1)S(1)}, bf16[1,320,896]{2,1,0:T(8,128)(2,1)}, u32[]{:S(2)}) copy-start(bf16[1,320,896]{2,1,0:T(8,128)(2,1)} %get-tuple-element.32) | copy-start | bytes 1720324
  140.3 34.8 %all-to-all-start.2 = ((bf16[8,2,15360]{2,1,0:T(2,128)(2,1)}), bf16[8,2,15360]{2,1,0:T(2,128)(2,1)S(1)}, u32[]{:S(2)}, u32[]{:S(2)}) async-start(bf16[8,2,15360]{2,1,0:T(2,128)(2,1)} %reshape.264), calls=%async_computation.2 | async-start | bytes 983040 | tf_op jit(solution)/shard_map/all_to_all | solution.py:74
  145.4 3.7 %copy-start.8 = (bf16[1,320,896]{2,1,0:T(8,128)(2,1)S(1)}, bf16[1,320,896]{2,1,0:T(8,128)(2,1)}, u32[]{:S(2)}) copy-start(bf16[1,320,896]{2,1,0:T(8,128)(2,1)} %get-tuple-element.33) | copy-start | bytes 1720324
  149.1 6.6 %copy-start.4 = (f32[128,2]{1,0:T(8,128)S(1)}, f32[128,2]{1,0:T(8,128)}, u32[]{:S(2)}) copy-start(f32[128,2]{1,0:T(8,128)} %copy-done.3) | copy-start | bytes 3076
Sparse Core Ops, SparseCore 0:
  59.5 62.4 all-reduce.2
Sparse Core Ops, SparseCore 1:
  62.7 32.3 reduce-scatter.1
